TPU v7x, 32 devices: a whole 2x2x4 slice. The times are simulated.
32 devices in a mesh: sp: 8 (over z, y), tp: 4 (over x, core).
Axes of the slice: x: 2, y: 2, z: 4, core: 2. Of those that a mesh axis runs over, the one named last changes fastest.
Arguments:
- query_nope: bfloat16 [1536, 4096], P('sp', 'tp'), may hold values from -6 to 6
- query_rope: bfloat16 [1536, 2048], P('sp', 'tp'), may hold values from -24 to 24
- latent: bfloat16 [1536, 512], P('sp'), may hold values from -6 to 6
- key_rope: bfloat16 [1536, 32], P('sp'), may hold values from -24 to 24
- latent_gain: float32 [512], replicated, may hold values from 0.1 to 1.9
- key_up: bfloat16 [512, 4096], P(None, 'tp'), may hold values from -0.25 to 0.25
- value_up: bfloat16 [512, 4096], P(None, 'tp'), may hold values from -0.25 to 0.25
- out_proj: bfloat16 [4096, 4096], P('tp'), may hold values from -0.09375 to 0.09375
- resid: bfloat16 [1536, 4096], P(('sp', 'tp')), may hold values from -6 to 6
- attn_gain: float32 [4096], replicated, may hold values from 0.1 to 1.9
- pre_gain: float32 [4096], replicated, may hold values from 0.1 to 1.9
- routes: int32 [1536, 2], P(('sp', 'tp')), may hold values from 0 to 7, all different within a row; in each aligned block of 48 rows (0 to 47, 48 to 95, ...) at most 24 rows name the same one
- route_weights: float32 [1536, 2], P(('sp', 'tp')), may hold values from 0.2 to 2
- expert_gate: bfloat16 [8, 4096, 1024], P('sp', None, 'tp'), may hold values from -0.09375 to 0.09375
- expert_up: bfloat16 [8, 4096, 1024], P('sp', None, 'tp'), may hold values from -0.09375 to 0.09375
- expert_down: bfloat16 [8, 1024, 4096], P('sp', 'tp'), may hold values from -0.1875 to 0.1875
- shared_gate: bfloat16 [4096, 1024], P(None, 'tp'), may hold values from -0.09375 to 0.09375
- shared_up: bfloat16 [4096, 1024], P(None, 'tp'), may hold values from -0.09375 to 0.09375
- shared_down: bfloat16 [1024, 4096], P('tp'), may hold values from -0.1875 to 0.1875
- moe_gain: float32 [4096], replicated, may hold values from 0.1 to 1.9
Outputs:
- output: bfloat16 [1536, 4096], P(('sp', 'tp'))
Inputs may be any that keep to these rules, and one draw needn't show every extreme that they name: `routes`: A row names 2 different experts. In each aligned block of 48 rows no expert is named by more than 24 rows, and in some block an expert is named by exactly 24 rows.
All inputs are finite; a program needn't handle non-finite values.
Results may differ from a plain program's by a relative error of at most 0.018.
Values may be sent and summed in bfloat16 or wider, within the bound.
A program may use at most 128 MiB of HBM per device.

v0:
```python
import math
import jax
import jax.numpy as jnp
from jax import lax
from jax.sharding import PartitionSpec as P

MODEL_DIM = 4096
NOPE_DIM = 64
ROPE_DIM = 32
VALUE_DIM = 64
TOP_K = 2
epsilon = 1e-06
theta_base = 10000.0


def rms_scale(values, gain_vector):
    return (
        values
        * lax.rsqrt(jnp.mean(values * values, axis=-1, keepdims=True) + epsilon)
        * gain_vector
    )


def rotate(values, positions):
    half_dim = values.shape[-1] // 2
    inverse = theta_base ** (-jnp.arange(half_dim, dtype=jnp.float32) / half_dim)
    angles = positions.astype(jnp.float32)[..., None] * inverse
    cosine = jnp.cos(angles)
    sine_part = jnp.sin(angles)
    first_half = values[..., :half_dim]
    second_half = values[..., half_dim:]
    return jnp.concatenate(
        [
            first_half * cosine - second_half * sine_part,
            second_half * cosine + first_half * sine_part,
        ],
        axis=-1,
    )


def expert_block(expert_in, gate_part, up_part, down_part):
    hidden = (
        jax.nn.silu(jnp.dot(expert_in, gate_part, preferred_element_type=jnp.float32))
        * jnp.dot(expert_in, up_part, preferred_element_type=jnp.float32)
    ).astype(jnp.bfloat16)
    return jnp.dot(hidden, down_part, preferred_element_type=jnp.float32).astype(jnp.bfloat16)


def dispatch_table(normed_rows, route_rows, experts, capacity):
    row_count = normed_rows.shape[0]
    flat_routes = route_rows.reshape(-1)
    onehot = (flat_routes[:, None] == jnp.arange(experts, dtype=jnp.int32)[None, :]).astype(
        jnp.int32
    )
    earlier = jnp.cumsum(onehot, axis=0) - onehot
    target = flat_routes * capacity + jnp.sum(earlier * onehot, axis=1)
    matches = (
        target.reshape(row_count, -1)[None, :, :]
        == jnp.arange(experts * capacity, dtype=jnp.int32)[:, None, None]
    )
    spread = jnp.any(matches, axis=2).astype(jnp.bfloat16)
    slot_table = jnp.dot(spread, normed_rows, preferred_element_type=jnp.float32).astype(
        jnp.bfloat16
    )
    return (slot_table.reshape(experts, capacity, normed_rows.shape[1]), target)


def on_device(
    query_nope,
    query_rope,
    latent,
    key_rope,
    latent_gain,
    key_up,
    value_up,
    out_proj,
    resid,
    attn_gain,
    pre_gain,
    routes,
    route_weights,
    expert_gate,
    expert_up,
    expert_down,
    shared_gate,
    shared_up,
    shared_down,
    moe_gain,
):
    local_rows = query_nope.shape[0]
    heads_here = query_nope.shape[1] // NOPE_DIM
    query_pos = lax.axis_index("sp") * local_rows + jnp.arange(local_rows, dtype=jnp.int32)
    last_query = lax.axis_index("sp") * local_rows + local_rows - 1
    query_rot = rotate(
        query_rope.astype(jnp.float32).reshape(local_rows, heads_here, ROPE_DIM), query_pos[:, None]
    ).astype(jnp.bfloat16)
    key_rot = rotate(key_rope.astype(jnp.float32), query_pos).astype(jnp.bfloat16)
    latent_normed = rms_scale(latent.astype(jnp.float32), latent_gain).astype(jnp.bfloat16)
    query_heads = query_nope.reshape(local_rows, heads_here, NOPE_DIM)
    score_scale = (NOPE_DIM + ROPE_DIM) ** (-0.5)

    def attend(state_now, latent_rows, rotary_rows, key_start):
        piece_rows = latent_rows.shape[0]
        keys_here = jnp.dot(latent_rows, key_up, preferred_element_type=jnp.float32).astype(
            jnp.bfloat16
        )
        keys_here = keys_here.reshape(piece_rows, heads_here, NOPE_DIM)
        values_here = jnp.dot(latent_rows, value_up, preferred_element_type=jnp.float32).astype(
            jnp.bfloat16
        )
        values_here = values_here.reshape(piece_rows, heads_here, VALUE_DIM)
        scores = (
            jnp.einsum("qhd,khd->hqk", query_heads, keys_here, preferred_element_type=jnp.float32)
            + jnp.einsum("qhr,kr->hqk", query_rot, rotary_rows, preferred_element_type=jnp.float32)
        ) * score_scale
        allowed = (key_start + jnp.arange(piece_rows, dtype=jnp.int32))[None, :] <= query_pos[
            :, None
        ]
        scores = jnp.where(allowed[None], scores, -1e30)
        running, total_sum, summed = state_now
        newest = jnp.maximum(running, jnp.max(scores, axis=-1))
        factor = jnp.exp(running - newest)
        exponent = jnp.exp(scores - newest[..., None])
        total_sum = total_sum * factor + jnp.sum(exponent, axis=-1)
        summed = summed * factor[..., None] + jnp.einsum(
            "hqk,khd->hqd",
            exponent.astype(jnp.bfloat16),
            values_here,
            preferred_element_type=jnp.float32,
        )
        return (newest, total_sum, summed)

    initial = (
        jnp.full((heads_here, local_rows), -1e30, jnp.float32),
        jnp.zeros((heads_here, local_rows), jnp.float32),
        jnp.zeros((heads_here, local_rows, VALUE_DIM), jnp.float32),
    )
    latent_piece = lax.all_gather(latent_normed, "sp", axis=0, tiled=True)
    rotary_piece = lax.all_gather(key_rot, "sp", axis=0, tiled=True)
    piece_rows = latent_piece.shape[0]
    step_rows = math.gcd(piece_rows, 512)

    def one_step(step_index, inner_state):
        offset = step_index * step_rows
        latent_rows = lax.dynamic_slice_in_dim(latent_piece, offset, step_rows, 0)
        rotary_rows = lax.dynamic_slice_in_dim(rotary_piece, offset, step_rows, 0)
        return lax.cond(
            offset <= last_query,
            lambda carried: attend(carried, latent_rows, rotary_rows, offset),
            lambda carried: carried,
            inner_state,
        )

    running, total_sum, summed = lax.fori_loop(0, piece_rows // step_rows, one_step, initial)
    attention = (
        (summed / total_sum[..., None])
        .transpose(1, 0, 2)
        .reshape(local_rows, heads_here * VALUE_DIM)
    )
    attention = attention.astype(jnp.bfloat16)
    projected = lax.psum_scatter(
        jnp.dot(attention, out_proj, preferred_element_type=jnp.float32).astype(jnp.bfloat16),
        "tp",
        scatter_dimension=0,
        tiled=True,
    ).astype(jnp.float32)
    mixed = (resid.astype(jnp.float32) + rms_scale(projected, attn_gain)).astype(jnp.bfloat16)
    normed = rms_scale(mixed.astype(jnp.float32), pre_gain).astype(jnp.bfloat16)
    rows_here = resid.shape[0]
    tp_count = lax.axis_size("tp")
    experts = lax.axis_size("sp")
    capacity = max(2, 2 * rows_here * TOP_K // experts)
    own_table, target = dispatch_table(normed, routes, experts, capacity)
    arrived = lax.all_to_all(own_table, "sp", split_axis=0, concat_axis=0, tiled=True)
    column = lax.all_gather(arrived[None], "tp", axis=0, tiled=True)
    group_normed = lax.all_gather(normed, "tp", axis=0, tiled=True)
    expert_out = expert_block(
        column.reshape(-1, MODEL_DIM), expert_gate[0], expert_up[0], expert_down[0]
    )
    shared_part = expert_block(group_normed, shared_gate, shared_up, shared_down)
    routed_sum, shared_sum = (
        lax.psum_scatter(
            expert_out.reshape(column.shape).astype(jnp.float32).astype(jnp.bfloat16),
            "tp",
            scatter_dimension=0,
            tiled=True,
        ).astype(jnp.float32),
        lax.psum_scatter(
            shared_part.reshape(tp_count, rows_here, MODEL_DIM)
            .astype(jnp.float32)
            .astype(jnp.bfloat16),
            "tp",
            scatter_dimension=0,
            tiled=True,
        ).astype(jnp.float32),
    )
    expert_rows = lax.all_to_all(
        routed_sum.astype(jnp.bfloat16), "sp", split_axis=1, concat_axis=1, tiled=True
    ).reshape(-1, MODEL_DIM)
    shared_out = shared_sum.reshape(rows_here, MODEL_DIM)
    picked = expert_rows[target].astype(jnp.float32).reshape(rows_here, TOP_K, MODEL_DIM)
    routed = jnp.sum(picked * route_weights[..., None], axis=1)
    moe = shared_out + routed
    return (mixed.astype(jnp.float32) + rms_scale(moe, moe_gain)).astype(jnp.bfloat16)


def solution(mesh):
    in_specs = (
        P("sp", "tp"),
        P("sp", "tp"),
        P("sp", None),
        P("sp", None),
        P(),
        P(None, "tp"),
        P(None, "tp"),
        P("tp", None),
        P(("sp", "tp"), None),
        P(),
        P(),
        P(("sp", "tp"), None),
        P(("sp", "tp"), None),
        P("sp", None, "tp"),
        P("sp", None, "tp"),
        P("sp", "tp", None),
        P(None, "tp"),
        P(None, "tp"),
        P("tp", None),
        P(),
    )
    out_specs = P(("sp", "tp"), None)
    return jax.shard_map(
        on_device, mesh=mesh, in_specs=in_specs, out_specs=out_specs, check_vma=False
    )
```

profile of v0, /device:TPU:0, one launch (start us, length us, event | category | flops | bytes accessed | tf_op | source)
XLA Modules:
  0.0 459.1 jit_solution(2781892771527778260)
XLA Ops:
  7.8 1.7 fusion.48
  11.5 32.8 %all-gather.1 = bf16[8,192,32]{1,2,0:T(8,128)(2,1)S(1)} all-gather(bf16[1,192,32]{1,2,0:T(8,128)(2,1)S(1)} %maximum_bitcast_fusion), channel_id=1, replica_groups=mesh['sp'=8,'tp'=4] {'sp'}, dimensions={0}, use_global_device_ids=true | all-gather | bytes 110592 | tf_op jit(solution)/shard_map/all_gather | solution.py:139
  46.3 10.5 %all-gather.6.cloned.1.call-done = bf16[1536,512]{1,0:T(8,128)(2,1)} async-done(((bf16[192,512]{1,0:T(8,128)(2,1)}), bf16[1536,512]{1,0:T(8,128)(2,1)}) %all-gather.6.cloned.1.call-update) | async-done | bytes 1572880 | tf_op jit(solution)/shard_map/all_gather | solution.py:138
  58.0 22.1 %while.18 = (s32[]{:T(128)}, f32[16,192]{1,0:T(8,128)S(1)}, f32[16,192]{1,0:T(8,128)S(1)}, f32[16,192,64]{1,2,0:T(8,128)}, s32[]{:T(128)}, /*index=5*/bf16[1536,...) while((s32[]{:T(128)}, f32[16,192]{1,0:T(8,128)S(1)}, ...), condition=%wide.region_6.7_spmd.clone, body=%wide.region_1.6_spmd.clone.sunk | while | flops 1591188224 | bytes 74948008 | solution.py:154
  58.0 22.1 %conditional.3 = ((f32[16,192]{1,0:T(8,128)S(1)}, f32[16,192]{1,0:T(8,128)S(1)}, f32[16,192,64]{1,2,0:T(8,128)})) conditional(s32[]{:T(128)} %convert_element_type.198, (f32[16,192]{1,0:T(8,128)S(1)}, f32[16,192]{1,0:T(8,128)S(1)}, f32[16,192,64]{1,2,0:T(8,128)}) %tuple.60, (s32[]{:T(128)}, s32[]{:T(128)}, bf16[1536,512]{1,0:T(8,128)(2,1)}, ...), branch_computations={%region_2.0_spmd, %region_3.5_spmd} | conditional | flops 1591188224 | bytes 74946960 | solution.py:147
  58.0 3.1 convolution_convert_fusion.1
  61.1 1.5 copy.63
  62.6 2.1 fusion.64
  64.8 2.9 fusion.63
  67.7 1.6 fusion.5
  70.3 2.8 convolution_convert_fusion
  73.1 1.5 copy.64
  74.6 5.4 %fusion.9 = f32[16,192,64]{1,2,0:T(8,128)} fusion(bf16[512,16,64]{0,2,1:T(8,128)(2,1)S(1)} %bitcast.74, f32[16,192,512]{2,1,0:T(8,128)} %copy-done.1, f32[16,192]{1,0:T(8,128)S(1)} %max.5, f32[16,192,64]{1,2,0:T(8,128)} %get-tuple-element.325, f32[16,192]{1,0:T(8,128)S(1)} %get-tuple-element.405), kind=kOutput, calls=%fused_computation.12 | convolution fusion | flops 204865536 | bytes 8937472 | tf_op jit(solution)/shard_map/while/body/eval_jaxpr/cond/branch_1_fun/hqk,khd->hqd/dot_general | solution.py:125
  80.1 1.3 divide_convert_fusion
  81.4 6.4 %convolution_convert_fusion.5 = bf16[192,4096]{1,0:T(8,128)(2,1)} fusion(bf16[192,1024]{0,1:T(8,128)(2,1)S(1)} %bitcast.80, bf16[1024,4096]{1,0:T(8,128)(2,1)} %param.31), kind=kOutput, calls=%fused_computation.28 | convolution fusion | flops 1611399168 | bytes 10354688 | tf_op jit(solution)/shard_map/dot_general | solution.py:162
  88.9 69.8 %reduce-scatter.4.cloned.1.call-done = bf16[48,4096]{1,0:T(8,128)(2,1)} async-done(((bf16[192,4096]{1,0:T(8,128)(2,1)}), bf16[48,4096]{1,0:T(8,128)(2,1)}) %reduce-scatter.4.cloned.1.call-update) | async-done | bytes 393232 | tf_op jit(solution)/shard_map/reduce_scatter | solution.py:161
  159.8 1.4 fusion.37
  162.0 42.3 %all_to_all.10 = bf16[8,24,4096]{2,1,0:T(8,128)(2,1)} all-to-all(bf16[8,24,4096]{2,1,0:T(8,128)(2,1)S(1)} %bitcast.79), channel_id=1, replica_groups=mesh['sp'=8,'tp'=4] {'sp'}, dimensions={0} | all-to-all | bytes 3145728 | tf_op jit(solution)/shard_map/all_to_all | solution.py:174
  205.1 43.8 %all-gather.10.cloned.1.call-done = bf16[32,24,4096]{2,1,0:T(8,128)(2,1)} async-done(((bf16[8,24,4096]{2,1,0:T(8,128)(2,1)}), bf16[32,24,4096]{2,1,0:T(8,128)(2,1)}) %all-gather.10.cloned.1.call-update) | async-done | bytes 6291472 | tf_op jit(solution)/shard_map/all_gather | solution.py:175
  248.9 6.1 %fusion.22 = f32[768,256]{1,0:T(8,128)} fusion(bf16[768,4096]{1,0:T(8,128)(2,1)} %bitcast.82, bf16[1,4096,256]{2,1,0:T(8,128)(2,1)} %param.37), kind=kOutput, calls=%fused_computation.32 | convolution fusion | flops 1610612736 | bytes 9175040 | tf_op jit(solution)/shard_map/dot_general | solution.py:43
  255.0 13.3 %convolution_convert_fusion.2 = bf16[768,4096]{1,0:T(8,128)(2,1)} fusion(bf16[1,256,4096]{2,1,0:T(8,128)(2,1)S(1)} %copy-done, bf16[768,4096]{1,0:T(8,128)(2,1)} %bitcast.83, bf16[1,4096,256]{2,1,0:T(8,128)(2,1)} %param.38, f32[768,256]{1,0:T(8,128)} %fusion.22), kind=kOutput, calls=%fused_computation.25 | convolution fusion | flops 3225550848 | bytes 17563648 | tf_op jit(solution)/shard_map/dot_general | solution.py:46
  268.2 6.3 %copy.71 = bf16[4,8,24,4096]{3,2,0,1:T(8,128)(2,1)} copy(bf16[4,8,24,4096]{3,2,1,0:T(8,128)(2,1)} %bitcast.77) | data formatting | bytes 12582912 | tf_op jit(solution)/shard_map/reshape | solution.py:183
  275.8 2.6 fusion.65
  278.4 6.9 %convolution_convert_fusion.4 = bf16[192,4096]{1,0:T(8,128)(2,1)} fusion(bf16[256,4096]{1,0:T(8,128)(2,1)} %param.42, bf16[192,4096]{1,0:T(8,128)(2,1)} %all-gather.8.cloned.1.call-done, bf16[4096,256]{1,0:T(8,128)(2,1)} %param.41, f32[192,256]{1,0:T(8,128)S(1)} %fusion.65), kind=kOutput, calls=%fused_computation.27 | convolution fusion | flops 806387712 | bytes 7536640 | tf_op jit(solution)/shard_map/dot_general | solution.py:46
  285.3 108.8 %all-reduce.3.cloned.1.call-done = bf16[4,8,24,4096]{3,2,0,1:T(8,128)(2,1)} async-done(((bf16[4,8,24,4096]{3,2,0,1:T(8,128)(2,1)}), bf16[4,8,24,4096]{3,2,0,1:T(8,128)(2,1)}) %all-reduce.3.cloned.1.call-update) | async-done | bytes 6291472
  394.2 3.3 constant_dynamic-slice_fusion
  397.5 5.6 %all-to-all-start.1 = ((bf16[1,8,24,4096]{3,2,0,1:T(8,128)(2,1)}), bf16[1,8,24,4096]{3,2,0,1:T(8,128)(2,1)}, u32[]{:S(2)}, u32[]{:S(2)}) async-start(bf16[1,8,24,4096]{3,2,0,1:T(8,128)(2,1)} %constant_dynamic-slice_fusion), calls=%async_computation.3 | async-start | bytes 3145728 | tf_op jit(solution)/shard_map/all_to_all | solution.py:197
  403.4 36.5 %all-to-all-done.1 = bf16[1,8,24,4096]{3,2,0,1:T(8,128)(2,1)} async-done(((bf16[1,8,24,4096]{3,2,0,1:T(8,128)(2,1)}), bf16[1,8,24,4096]{3,2,0,1:T(8,128)(2,1)}, u32[]{:S(2)}, u32[]{:S(2)}) %all-to-all-start.1) | async-done | bytes 1572896 | tf_op jit(solution)/shard_map/all_to_all | solution.py:197
  439.8 3.4 gather_fusion
  443.2 2.1 reshape.251
  445.4 3.6 multiply_reduce_fusion
  450.3 1.9 fusion.40
  (86 shorter events, 14.0 us)
Async XLA Ops:
  6.5 248.4 %copy-start = (bf16[1,256,4096]{2,1,0:T(8,128)(2,1)S(1)}, bf16[1,256,4096]{2,1,0:T(8,128)(2,1)}, u32[]{:S(2)}) copy-start(bf16[1,256,4096]{2,1,0:T(8,128)(2,1)} %param.39) | copy-start | bytes 6291460
  6.5 38.6 %copy-start.3 = (bf16[192,1024]{1,0:T(8,128)(2,1)S(1)}, bf16[192,1024]{1,0:T(8,128)(2,1)}, u32[]{:S(2)}) copy-start(bf16[192,1024]{1,0:T(8,128)(2,1)} %param.24) | copy-start | bytes 1179652
  6.5 50.3 %all-gather.6.cloned.1.call-start = ((), (), s32[]{:S(2)}) async-start(), calls=%async_computation.4 | async-start | bytes 1769472 | tf_op jit(solution)/shard_map/all_gather | solution.py:138
  9.5 149.1 %reduce-scatter.4.cloned.1.call-start = ((), (), s32[]{:S(2)}) async-start(), calls=%async_computation.5 | async-start | bytes 1966080 | tf_op jit(solution)/shard_map/reduce_scatter | solution.py:161
  67.7 2.6 copy-start.1
  67.7 2.6 copy-start.10
  81.4 6.5 %copy-start.8 = (s32[48,2]{0,1:T(2,128)S(1)}, s32[48,2]{0,1:T(2,128)}, u32[]{:S(2)}) copy-start(s32[48,2]{0,1:T(2,128)} %param.35) | copy-start | bytes 1156
  87.8 72.0 %copy-start.4 = (bf16[48,4096]{1,0:T(8,128)(2,1)S(1)}, bf16[48,4096]{1,0:T(8,128)(2,1)}, u32[]{:S(2)}) copy-start(bf16[48,4096]{1,0:T(8,128)(2,1)} %param.32) | copy-start | bytes 1179652
  87.8 72.0 %copy-start.5 = (f32[4096]{0:T(1024)S(1)}, f32[4096]{0:T(1024)}, u32[]{:S(2)}) copy-start(f32[4096]{0:T(1024)} %param.33) | copy-start | bytes 49156
  87.8 73.4 %copy-start.7 = (f32[4096]{0:T(1024)S(1)}, f32[4096]{0:T(1024)}, u32[]{:S(2)}) copy-start(f32[4096]{0:T(1024)} %param.34) | copy-start | bytes 49156
  87.9 161.0 %all-gather.10.cloned.1.call-start = ((), (), s32[]{:S(2)}) async-start(), calls=%async_computation.8 | async-start | bytes 7864320 | tf_op jit(solution)/shard_map/all_gather | solution.py:175
  161.4 42.9 %copy-start.2 = (bf16[48,4096]{1,0:T(8,128)(2,1)}, bf16[48,4096]{1,0:T(8,128)(2,1)S(1)}, u32[]{:S(2)}) copy-start(bf16[48,4096]{1,0:T(8,128)(2,1)S(1)} %fusion.39) | copy-start | bytes 1179652
  204.3 71.5 %all-gather.8.cloned.1.call-start = ((), (), s32[]{:S(2)}) async-start(), calls=%async_computation.6 | async-start | bytes 1966080 | tf_op jit(solution)/shard_map/all_gather | solution.py:176
  204.9 189.3 %all-reduce.3.cloned.1.call-start = ((), (), s32[]{:S(2)}) async-start(), calls=%async_computation.9 | async-start | bytes 12582912
  274.5 0.7 copy-start.11
  274.5 174.5 %reduce-scatter.6.cloned.1.call-start = ((), (), s32[]{:S(2)}) async-start(), calls=%async_computation.7 | async-start | bytes 1966080 | tf_op jit(solution)/shard_map/reduce_scatter | solution.py:188
  397.5 5.8 %copy-start.9 = (f32[48,2]{0,1:T(2,128)S(1)}, f32[48,2]{0,1:T(2,128)}, u32[]{:S(2)}) copy-start(f32[48,2]{0,1:T(2,128)} %param.36) | copy-start | bytes 1156
  397.5 42.4 %all-to-all-start.1 = ((bf16[1,8,24,4096]{3,2,0,1:T(8,128)(2,1)}), bf16[1,8,24,4096]{3,2,0,1:T(8,128)(2,1)}, u32[]{:S(2)}, u32[]{:S(2)}) async-start(bf16[1,8,24,4096]{3,2,0,1:T(8,128)(2,1)} %constant_dynamic-slice_fusion), calls=%async_computation.3 | async-start | bytes 3145728 | tf_op jit(solution)/shard_map/all_to_all | solution.py:197
  445.4 4.9 %copy-start.6 = (f32[4096]{0:T(1024)S(1)}, f32[4096]{0:T(1024)}, u32[]{:S(2)}) copy-start(f32[4096]{0:T(1024)} %param.43) | copy-start | bytes 49156
Sparse Core Ops, SparseCore 0:
  9.6 47.1 all-gather.5
  88.0 70.5 reduce-scatter.3
  204.4 44.4 all-gather.9
  250.3 19.6 all-gather.7
  274.6 119.4 all-reduce.2
  396.5 28.2 reduce-scatter.5
where the time goes:
time: 460 us; the launch traced here: 459 us
  waiting for transfers between devices  270 us (59%)
  blocking collectives  75 us (16%)
  matrix products  52.1 us (11%)
  local copies, waits for them, and re-layouts  25 us (5%)
  other arithmetic  17.1 us (4%)
  between operations  13.7 us (3%)
  starting transfers between devices  6.04 us (1%)
    unnamed x7, waiting for transfers between devices  109 us
    reduce_scatter x1, waiting for transfers between devices, on_device(): lax.psum_scatter(jnp.dot(attention, out_proj, preferred_element_type=jnp....  69.8 us
    all_gather x1, waiting for transfers between devices, on_device(): column = lax.all_gather(arrived[None], 'tp', axis=0, tiled=True)  43.8 us
    all_to_all x1, blocking collectives, on_device(): lax.all_to_all(own_table, 'sp', split_axis=0, concat_axis=0, tiled=True)  42.3 us
    all_to_all x1, waiting for transfers between devices, on_device(): lax.all_to_all(routed_sum.astype(jnp.bfloat16), 'sp', split_axis=1, conca...  36.5 us
    all_gather x1, blocking collectives, on_device(): rotary_piece = lax.all_gather(key_rot, 'sp', axis=0, tiled=True)  32.8 us
    dot_general x2, matrix products, expert_block(): jnp.dot(hidden, down_part, preferred_element_type=jnp.float32)  20.1 us
    all_gather x1, waiting for transfers between devices, on_device(): latent_piece = lax.all_gather(latent_normed, 'sp', axis=0, tiled=True)  10.5 us
  transfers between devices with their start and end apart: 7, of which 5 were waited for; matrix products, arithmetic and copies ran while one was open for 12% of the time, Pallas kernels for 0%

commit v1 on v0

--- a/solution.py
+++ b/solution.py
@@ -136,7 +136,12 @@
         jnp.zeros((heads_here, local_rows, VALUE_DIM), jnp.float32),
     )
     latent_piece = lax.all_gather(latent_normed, "sp", axis=0, tiled=True)
-    rotary_piece = lax.all_gather(key_rot, "sp", axis=0, tiled=True)
+    ring = [key_rot]
+    for hop in range(7):
+        ring.append(lax.ppermute(ring[-1], "sp", [(dev, (dev + 1) % 8) for dev in range(8)]))
+    rotary_piece = jnp.roll(
+        jnp.concatenate(ring[::-1], axis=0), (lax.axis_index("sp") + 1) * ring[0].shape[0], axis=0
+    )
     piece_rows = latent_piece.shape[0]
     step_rows = math.gcd(piece_rows, 512)
 

time: 460 us -> 461 us (level)
  blocking collectives: 75 us -> 42.3 us
  waiting for transfers between devices: 270 us -> 299 us
    ppermute x0 -> x7, waiting for transfers between devices: none -> 41 us  [on_device(): lax.ppermute(ring[-1], 'sp', [(dev, (dev + 1) % 8) for dev in range(8)])]
    all_gather x1 -> x0, blocking collectives: 32.8 us -> none  [on_device(): rotary_piece = lax.all_gather(key_rot, 'sp', axis=0, tiled=True)]
    all_gather x1, waiting for transfers between devices: 10.5 us -> 0.01 us  [on_device(): latent_piece = lax.all_gather(latent_normed, 'sp', axis=0, tiled=True)]
  transfers between devices with their start and end apart: 7 -> 14, of which waited for: 5 -> 11; matrix products, arithmetic and copies ran while one was open for 12% -> 12% of each run, Pallas kernels for 0% -> 0%
where the time goes in v1:
time: 461 us; the launch traced here: 459 us
  waiting for transfers between devices  299 us (65%)
  matrix products  52 us (11%)
  blocking collectives  42.3 us (9%)
  local copies, waits for them, and re-layouts  26.1 us (6%)
  other arithmetic  17 us (4%)
  between operations  13.8 us (3%)
  starting transfers between devices  9.1 us (2%)
    unnamed x7, waiting for transfers between devices  110 us
    reduce_scatter x1, waiting for transfers between devices, on_device(): lax.psum_scatter(jnp.dot(attention, out_proj, preferred_element_type=jnp....  68.1 us
    all_gather x1, waiting for transfers between devices, on_device(): column = lax.all_gather(arrived[None], 'tp', axis=0, tiled=True)  43.8 us
    all_to_all x1, blocking collectives, on_device(): lax.all_to_all(own_table, 'sp', split_axis=0, concat_axis=0, tiled=True)  42.3 us
    ppermute x7, waiting for transfers between devices, on_device(): lax.ppermute(ring[-1], 'sp', [(dev, (dev + 1) % 8) for dev in range(8)])  41 us
    all_to_all x1, waiting for transfers between devices, on_device(): lax.all_to_all(routed_sum.astype(jnp.bfloat16), 'sp', split_axis=1, conca...  36.5 us
    dot_general x2, matrix products, expert_block(): jnp.dot(hidden, down_part, preferred_element_type=jnp.float32)  20.1 us
  transfers between devices with their start and end apart: 14, of which 11 were waited for; matrix products, arithmetic and copies ran while one was open for 12% of the time, Pallas kernels for 0%

profile of v1, /device:TPU:0, one launch (start us, length us, event | category | flops | bytes accessed | tf_op | source)
XLA Modules:
  0.0 459.3 jit_solution(56015200580845666)
XLA Ops:
  10.5 3.0 collective-permute-start
  13.5 4.8 %collective-permute-done = bf16[192,32]{0,1:T(8,128)(2,1)S(1)} collective-permute-done((bf16[192,32]{0,1:T(8,128)(2,1)S(1)}, bf16[192,32]{0,1:T(8,128)(2,1)S(1)}, u32[]{:S(2)}, u32[]{:S(2)}) %collective-permute-start) | collective-permute-done | bytes 12320 | tf_op jit(solution)/shard_map/ppermute | solution.py:141
  18.3 6.5 %collective-permute-done.1 = bf16[192,32]{0,1:T(8,128)(2,1)S(1)} collective-permute-done((bf16[192,32]{0,1:T(8,128)(2,1)S(1)}, bf16[192,32]{0,1:T(8,128)(2,1)S(1)}, u32[]{:S(2)}, u32[]{:S(2)}) %collective-permute-start.1) | collective-permute-done | bytes 12320 | tf_op jit(solution)/shard_map/ppermute | solution.py:141
  24.8 6.5 %collective-permute-done.2 = bf16[192,32]{0,1:T(8,128)(2,1)S(1)} collective-permute-done((bf16[192,32]{0,1:T(8,128)(2,1)S(1)}, bf16[192,32]{0,1:T(8,128)(2,1)S(1)}, u32[]{:S(2)}, u32[]{:S(2)}) %collective-permute-start.2) | collective-permute-done | bytes 12320 | tf_op jit(solution)/shard_map/ppermute | solution.py:141
  31.3 6.4 %collective-permute-done.3 = bf16[192,32]{0,1:T(8,128)(2,1)S(1)} collective-permute-done((bf16[192,32]{0,1:T(8,128)(2,1)S(1)}, bf16[192,32]{0,1:T(8,128)(2,1)S(1)}, u32[]{:S(2)}, u32[]{:S(2)}) %collective-permute-start.3) | collective-permute-done | bytes 12320 | tf_op jit(solution)/shard_map/ppermute | solution.py:141
  38.9 5.7 %collective-permute-done.4 = bf16[192,32]{0,1:T(8,128)(2,1)S(1)} collective-permute-done((bf16[192,32]{0,1:T(8,128)(2,1)S(1)}, bf16[192,32]{0,1:T(8,128)(2,1)S(1)}, u32[]{:S(2)}, u32[]{:S(2)}) %collective-permute-start.4) | collective-permute-done | bytes 12320 | tf_op jit(solution)/shard_map/ppermute | solution.py:141
  44.6 6.4 %collective-permute-done.5 = bf16[192,32]{0,1:T(8,128)(2,1)S(1)} collective-permute-done((bf16[192,32]{0,1:T(8,128)(2,1)S(1)}, bf16[192,32]{0,1:T(8,128)(2,1)S(1)}, u32[]{:S(2)}, u32[]{:S(2)}) %collective-permute-start.5) | collective-permute-done | bytes 12320 | tf_op jit(solution)/shard_map/ppermute | solution.py:141
  51.1 2.0 copy.53
  53.1 4.6 %collective-permute-done.6 = bf16[192,32]{0,1:T(8,128)(2,1)S(1)} collective-permute-done((bf16[192,32]{0,1:T(8,128)(2,1)S(1)}, bf16[192,32]{0,1:T(8,128)(2,1)S(1)}, u32[]{:S(2)}, u32[]{:S(2)}) %collective-permute-start.6) | collective-permute-done | bytes 12320 | tf_op jit(solution)/shard_map/ppermute | solution.py:141
  59.8 22.1 %while.18 = (s32[]{:T(128)}, f32[16,192]{1,0:T(8,128)S(1)}, f32[16,192]{1,0:T(8,128)S(1)}, f32[16,192,64]{1,2,0:T(8,128)}, s32[]{:T(128)}, /*index=5*/bf16[1536,...) while((s32[]{:T(128)}, f32[16,192]{1,0:T(8,128)S(1)}, ...), condition=%wide.region_6.7_spmd.clone, body=%wide.region_1.6_spmd.clone.sunk | while | flops 1591188224 | bytes 74948008 | solution.py:159
  59.8 22.1 %conditional.3 = ((f32[16,192]{1,0:T(8,128)S(1)}, f32[16,192]{1,0:T(8,128)S(1)}, f32[16,192,64]{1,2,0:T(8,128)})) conditional(s32[]{:T(128)} %convert_element_type.198, (f32[16,192]{1,0:T(8,128)S(1)}, f32[16,192]{1,0:T(8,128)S(1)}, f32[16,192,64]{1,2,0:T(8,128)}) %tuple.60, (s32[]{:T(128)}, s32[]{:T(128)}, bf16[1536,512]{1,0:T(8,128)(2,1)}, ...), branch_computations={%region_2.2_spmd, %region_3.5_spmd} | conditional | flops 1591188224 | bytes 74946960 | solution.py:152
  59.8 3.1 convolution_convert_fusion.1
  64.4 2.1 fusion.64
  66.6 2.9 fusion.63
  72.2 2.7 convolution_convert_fusion
  76.4 5.4 %fusion.9 = f32[16,192,64]{1,2,0:T(8,128)} fusion(bf16[512,16,64]{0,2,1:T(8,128)(2,1)S(1)} %bitcast.70, f32[16,192,512]{2,1,0:T(8,128)} %copy-done.1, f32[16,192]{1,0:T(8,128)S(1)} %max.5, f32[16,192,64]{1,2,0:T(8,128)} %get-tuple-element.325, f32[16,192]{1,0:T(8,128)S(1)} %get-tuple-element.405), kind=kOutput, calls=%fused_computation.12 | convolution fusion | flops 204865536 | bytes 8937472 | tf_op jit(solution)/shard_map/while/body/eval_jaxpr/cond/branch_1_fun/hqk,khd->hqd/dot_general | solution.py:125
  83.3 6.4 %convolution_convert_fusion.5 = bf16[192,4096]{1,0:T(8,128)(2,1)} fusion(bf16[192,1024]{0,1:T(8,128)(2,1)S(1)} %bitcast.76, bf16[1024,4096]{1,0:T(8,128)(2,1)} %param.31), kind=kOutput, calls=%fused_computation.28 | convolution fusion | flops 1611399168 | bytes 10354688 | tf_op jit(solution)/shard_map/dot_general | solution.py:167
  90.7 68.1 %reduce-scatter.4.cloned.1.call-done = bf16[48,4096]{1,0:T(8,128)(2,1)} async-done(((bf16[192,4096]{1,0:T(8,128)(2,1)}), bf16[48,4096]{1,0:T(8,128)(2,1)}) %reduce-scatter.4.cloned.1.call-update) | async-done | bytes 393232 | tf_op jit(solution)/shard_map/reduce_scatter | solution.py:166
  162.2 42.3 %all_to_all.10 = bf16[8,24,4096]{2,1,0:T(8,128)(2,1)} all-to-all(bf16[8,24,4096]{2,1,0:T(8,128)(2,1)S(1)} %bitcast.75), channel_id=1, replica_groups=mesh['sp'=8,'tp'=4] {'sp'}, dimensions={0} | all-to-all | bytes 3145728 | tf_op jit(solution)/shard_map/all_to_all | solution.py:179
  205.3 43.8 %all-gather.9.cloned.1.call-done = bf16[32,24,4096]{2,1,0:T(8,128)(2,1)} async-done(((bf16[8,24,4096]{2,1,0:T(8,128)(2,1)}), bf16[32,24,4096]{2,1,0:T(8,128)(2,1)}) %all-gather.9.cloned.1.call-update) | async-done | bytes 6291472 | tf_op jit(solution)/shard_map/all_gather | solution.py:180
  249.0 6.1 %fusion.22 = f32[768,256]{1,0:T(8,128)} fusion(bf16[768,4096]{1,0:T(8,128)(2,1)} %bitcast.78, bf16[1,4096,256]{2,1,0:T(8,128)(2,1)} %param.37), kind=kOutput, calls=%fused_computation.32 | convolution fusion | flops 1610612736 | bytes 9175040 | tf_op jit(solution)/shard_map/dot_general | solution.py:43
  255.1 13.3 %convolution_convert_fusion.2 = bf16[768,4096]{1,0:T(8,128)(2,1)} fusion(bf16[1,256,4096]{2,1,0:T(8,128)(2,1)S(1)} %copy-done, bf16[768,4096]{1,0:T(8,128)(2,1)} %bitcast.79, bf16[1,4096,256]{2,1,0:T(8,128)(2,1)} %param.38, f32[768,256]{1,0:T(8,128)} %fusion.22), kind=kOutput, calls=%fused_computation.25 | convolution fusion | flops 3225550848 | bytes 17563648 | tf_op jit(solution)/shard_map/dot_general | solution.py:46
  268.4 6.2 %copy.58 = bf16[4,8,24,4096]{3,2,0,1:T(8,128)(2,1)} copy(bf16[4,8,24,4096]{3,2,1,0:T(8,128)(2,1)} %bitcast.73) | data formatting | bytes 12582912 | tf_op jit(solution)/shard_map/reshape | solution.py:188
  275.9 2.6 fusion.65
  278.6 6.8 %convolution_convert_fusion.4 = bf16[192,4096]{1,0:T(8,128)(2,1)} fusion(bf16[256,4096]{1,0:T(8,128)(2,1)} %param.42, bf16[192,4096]{1,0:T(8,128)(2,1)} %all-gather.7.cloned.1.call-done, bf16[4096,256]{1,0:T(8,128)(2,1)} %param.41, f32[192,256]{1,0:T(8,128)S(1)} %fusion.65), kind=kOutput, calls=%fused_computation.27 | convolution fusion | flops 806387712 | bytes 7536640 | tf_op jit(solution)/shard_map/dot_general | solution.py:46
  285.4 108.9 %all-reduce.3.cloned.1.call-done = bf16[4,8,24,4096]{3,2,0,1:T(8,128)(2,1)} async-done(((bf16[4,8,24,4096]{3,2,0,1:T(8,128)(2,1)}), bf16[4,8,24,4096]{3,2,0,1:T(8,128)(2,1)}) %all-reduce.3.cloned.1.call-update) | async-done | bytes 6291472
  394.3 3.3 constant_dynamic-slice_fusion
  397.7 5.6 %all-to-all-start.1 = ((bf16[1,8,24,4096]{3,2,0,1:T(8,128)(2,1)}), bf16[1,8,24,4096]{3,2,0,1:T(8,128)(2,1)}, u32[]{:S(2)}, u32[]{:S(2)}) async-start(bf16[1,8,24,4096]{3,2,0,1:T(8,128)(2,1)} %constant_dynamic-slice_fusion), calls=%async_computation.3 | async-start | bytes 3145728 | tf_op jit(solution)/shard_map/all_to_all | solution.py:202
  403.6 36.5 %all-to-all-done.1 = bf16[1,8,24,4096]{3,2,0,1:T(8,128)(2,1)} async-done(((bf16[1,8,24,4096]{3,2,0,1:T(8,128)(2,1)}), bf16[1,8,24,4096]{3,2,0,1:T(8,128)(2,1)}, u32[]{:S(2)}, u32[]{:S(2)}) %all-to-all-start.1) | async-done | bytes 1572896 | tf_op jit(solution)/shard_map/all_to_all | solution.py:202
  440.0 3.4 gather_fusion
  443.4 2.1 reshape.251
  445.6 3.6 multiply_reduce_fusion
  (97 shorter events, 24.0 us)
Async XLA Ops:
  6.5 248.6 %copy-start = (bf16[1,256,4096]{2,1,0:T(8,128)(2,1)S(1)}, bf16[1,256,4096]{2,1,0:T(8,128)(2,1)}, u32[]{:S(2)}) copy-start(bf16[1,256,4096]{2,1,0:T(8,128)(2,1)} %param.39) | copy-start | bytes 6291460
  6.5 52.1 %all-gather.5.cloned.1.call-start = ((), (), s32[]{:S(2)}) async-start(), calls=%async_computation.4 | async-start | bytes 1769472 | tf_op jit(solution)/shard_map/all_gather | solution.py:138
  9.5 149.3 %reduce-scatter.4.cloned.1.call-start = ((), (), s32[]{:S(2)}) async-start(), calls=%async_computation.5 | async-start | bytes 1966080 | tf_op jit(solution)/shard_map/reduce_scatter | solution.py:166
  10.5 7.8 %collective-permute-start = (bf16[192,32]{0,1:T(8,128)(2,1)S(1)}, bf16[192,32]{0,1:T(8,128)(2,1)S(1)}, u32[]{:S(2)}, u32[]{:S(2)}) collective-permute-start(bf16[192,32]{0,1:T(8,128)(2,1)S(1)} %pad_maximum_fusion.1), channel_id=1, source_target_pairs={{0,4},{4,8},{8,12},{12,16},{16,20},{20,24},{24,28},{28,0},{1,5},{5... | collective-permute-start | bytes 36872 | tf_op jit(solution)/shard_map/ppermute | solution.py:141
  18.3 6.5 %collective-permute-start.1 = (bf16[192,32]{0,1:T(8,128)(2,1)S(1)}, bf16[192,32]{0,1:T(8,128)(2,1)S(1)}, u32[]{:S(2)}, u32[]{:S(2)}) collective-permute-start(bf16[192,32]{0,1:T(8,128)(2,1)S(1)} %collective-permute-done), channel_id=1, source_target_pairs={{0,4},{4,8},{8,12},{12,16},{16,20},{20,24},{24,28},{28,0},{1,5},{5... | collective-permute-start | bytes 36872 | tf_op jit(solution)/shard_map/ppermute | solution.py:141
  24.8 6.5 %collective-permute-start.2 = (bf16[192,32]{0,1:T(8,128)(2,1)S(1)}, bf16[192,32]{0,1:T(8,128)(2,1)S(1)}, u32[]{:S(2)}, u32[]{:S(2)}) collective-permute-start(bf16[192,32]{0,1:T(8,128)(2,1)S(1)} %collective-permute-done.1), channel_id=1, source_target_pairs={{0,4},{4,8},{8,12},{12,16},{16,20},{20,24},{24,28},{28,0},{1,5},{5... | collective-permute-start | bytes 36872 | tf_op jit(solution)/shard_map/ppermute | solution.py:141
  31.3 6.4 %collective-permute-start.3 = (bf16[192,32]{0,1:T(8,128)(2,1)S(1)}, bf16[192,32]{0,1:T(8,128)(2,1)S(1)}, u32[]{:S(2)}, u32[]{:S(2)}) collective-permute-start(bf16[192,32]{0,1:T(8,128)(2,1)S(1)} %collective-permute-done.2), channel_id=1, source_target_pairs={{0,4},{4,8},{8,12},{12,16},{16,20},{20,24},{24,28},{28,0},{1,5},{5... | collective-permute-start | bytes 36872 | tf_op jit(solution)/shard_map/ppermute | solution.py:141
  37.8 6.8 %collective-permute-start.4 = (bf16[192,32]{0,1:T(8,128)(2,1)S(1)}, bf16[192,32]{0,1:T(8,128)(2,1)S(1)}, u32[]{:S(2)}, u32[]{:S(2)}) collective-permute-start(bf16[192,32]{0,1:T(8,128)(2,1)S(1)} %collective-permute-done.3), channel_id=1, source_target_pairs={{0,4},{4,8},{8,12},{12,16},{16,20},{20,24},{24,28},{28,0},{1,5},{5... | collective-permute-start | bytes 36872 | tf_op jit(solution)/shard_map/ppermute | solution.py:141
  44.5 6.5 %collective-permute-start.5 = (bf16[192,32]{0,1:T(8,128)(2,1)S(1)}, bf16[192,32]{0,1:T(8,128)(2,1)S(1)}, u32[]{:S(2)}, u32[]{:S(2)}) collective-permute-start(bf16[192,32]{0,1:T(8,128)(2,1)S(1)} %collective-permute-done.4), channel_id=1, source_target_pairs={{0,4},{4,8},{8,12},{12,16},{16,20},{20,24},{24,28},{28,0},{1,5},{5... | collective-permute-start | bytes 36872 | tf_op jit(solution)/shard_map/ppermute | solution.py:141
  51.1 6.7 %collective-permute-start.6 = (bf16[192,32]{0,1:T(8,128)(2,1)S(1)}, bf16[192,32]{0,1:T(8,128)(2,1)S(1)}, u32[]{:S(2)}, u32[]{:S(2)}) collective-permute-start(bf16[192,32]{0,1:T(8,128)(2,1)S(1)} %collective-permute-done.5), channel_id=1, source_target_pairs={{0,4},{4,8},{8,12},{12,16},{16,20},{20,24},{24,28},{28,0},{1,5},{5... | collective-permute-start | bytes 36872 | tf_op jit(solution)/shard_map/ppermute | solution.py:141
  69.5 2.7 copy-start.1
  69.5 2.7 copy-start.9
  83.2 6.5 %copy-start.7 = (s32[48,2]{0,1:T(2,128)S(1)}, s32[48,2]{0,1:T(2,128)}, u32[]{:S(2)}) copy-start(s32[48,2]{0,1:T(2,128)} %param.35) | copy-start | bytes 1156
  89.6 70.3 %copy-start.3 = (bf16[48,4096]{1,0:T(8,128)(2,1)S(1)}, bf16[48,4096]{1,0:T(8,128)(2,1)}, u32[]{:S(2)}) copy-start(bf16[48,4096]{1,0:T(8,128)(2,1)} %param.32) | copy-start | bytes 1179652
  89.6 70.3 %copy-start.4 = (f32[4096]{0:T(1024)S(1)}, f32[4096]{0:T(1024)}, u32[]{:S(2)}) copy-start(f32[4096]{0:T(1024)} %param.33) | copy-start | bytes 49156
  89.6 71.7 %copy-start.6 = (f32[4096]{0:T(1024)S(1)}, f32[4096]{0:T(1024)}, u32[]{:S(2)}) copy-start(f32[4096]{0:T(1024)} %param.34) | copy-start | bytes 49156
  89.7 159.4 %all-gather.9.cloned.1.call-start = ((), (), s32[]{:S(2)}) async-start(), calls=%async_computation.8 | async-start | bytes 7864320 | tf_op jit(solution)/shard_map/all_gather | solution.py:180
  161.5 42.9 %copy-start.2 = (bf16[48,4096]{1,0:T(8,128)(2,1)}, bf16[48,4096]{1,0:T(8,128)(2,1)S(1)}, u32[]{:S(2)}) copy-start(bf16[48,4096]{1,0:T(8,128)(2,1)S(1)} %fusion.39) | copy-start | bytes 1179652
  204.5 71.5 %all-gather.7.cloned.1.call-start = ((), (), s32[]{:S(2)}) async-start(), calls=%async_computation.6 | async-start | bytes 1966080 | tf_op jit(solution)/shard_map/all_gather | solution.py:181
  205.0 189.3 %all-reduce.3.cloned.1.call-start = ((), (), s32[]{:S(2)}) async-start(), calls=%async_computation.9 | async-start | bytes 12582912
  274.7 0.7 copy-start.10
  274.7 174.5 %reduce-scatter.6.cloned.1.call-start = ((), (), s32[]{:S(2)}) async-start(), calls=%async_computation.7 | async-start | bytes 1966080 | tf_op jit(solution)/shard_map/reduce_scatter | solution.py:193
  397.7 5.8 %copy-start.8 = (f32[48,2]{0,1:T(2,128)S(1)}, f32[48,2]{0,1:T(2,128)}, u32[]{:S(2)}) copy-start(f32[48,2]{0,1:T(2,128)} %param.36) | copy-start | bytes 1156
  397.7 42.4 %all-to-all-start.1 = ((bf16[1,8,24,4096]{3,2,0,1:T(8,128)(2,1)}), bf16[1,8,24,4096]{3,2,0,1:T(8,128)(2,1)}, u32[]{:S(2)}, u32[]{:S(2)}) async-start(bf16[1,8,24,4096]{3,2,0,1:T(8,128)(2,1)} %constant_dynamic-slice_fusion), calls=%async_computation.3 | async-start | bytes 3145728 | tf_op jit(solution)/shard_map/all_to_all | solution.py:202
  445.6 4.9 %copy-start.5 = (f32[4096]{0:T(1024)S(1)}, f32[4096]{0:T(1024)}, u32[]{:S(2)}) copy-start(f32[4096]{0:T(1024)} %param.43) | copy-start | bytes 49156
Sparse Core Ops, SparseCore 0:
  9.6 46.8 all-gather.4
  89.8 68.9 reduce-scatter.3
  204.6 44.4 all-gather.8
  250.5 19.6 all-gather.6
  274.8 119.4 all-reduce.2
  396.7 28.2 reduce-scatter.5
